TPU v7x, 128 devices: a whole 4x4x4 slice. The times are simulated.
128 devices in a mesh: rep: 2 (over z_hi), fs: 32 (over z_lo, y, x), tp: 2 (over core).
Axes of the slice: x: 4, y: 4, z: 4 (z_hi: 2, z_lo: 2; z = z_hi * 2 + z_lo), core: 2. Of those that a mesh axis runs over, the one named last changes fastest.
Arguments:
- sequence: bfloat16 [64, 768, 2048], P(('rep', 'fs'), None, 'tp'), may hold values from -6 to 6
- mix_gain: float32 [2048], replicated, may hold values from 0.1 to 1.9
- ffn_gain: float32 [2048], replicated, may hold values from 0.1 to 1.9
- proj_outer: float32 [2048, 2048], P(None, ('tp', 'fs')), may hold values from -0.125 to 0.125
- proj_inner: float32 [2048, 2048], P(None, ('tp', 'fs')), may hold values from -0.125 to 0.125
- proj_value: float32 [2048, 2048], P(None, ('tp', 'fs')), may hold values from -0.125 to 0.125
- proj_scales: float32 [3, 2048], P(None, 'tp'), may hold values from 0.5 to 2
- taps: float32 [3, 2048], P(None, 'tp'), may hold values from -3 to 3
- mix_out: float32 [2048, 2048], P('tp', 'fs'), may hold values from -0.125 to 0.125
- mix_out_scale: float32 [2048], P('fs'), may hold values from 0.5 to 2
- ffn_gate: float32 [2048, 2816], P(None, ('tp', 'fs')), may hold values from -0.125 to 0.125
- ffn_up: float32 [2048, 2816], P(None, ('tp', 'fs')), may hold values from -0.125 to 0.125
- ffn_scales: float32 [2, 2816], P(None, 'tp'), may hold values from 0.5 to 2
- ffn_down: float32 [2816, 2048], P('tp', 'fs'), may hold values from -0.109375 to 0.109375
- down_scale: float32 [2048], P('fs'), may hold values from 0.5 to 2
Outputs:
- layer_out: bfloat16 [64, 768, 2048], P(('rep', 'fs'), None, 'tp')
All inputs are finite; a program needn't handle non-finite values.
Results may differ from a plain program's by a relative error of at most 0.013.
Values may be sent and summed in bfloat16 or wider, within the bound.
A program may use at most 128 MiB of HBM per device.

v0:
```python
import jax
import jax.numpy as jnp
from jax import lax
from jax.sharding import PartitionSpec as P

eps = 1e-06


def gather_turned(arrays, axis, dims):
    turned = [jnp.moveaxis(a, dim, 0) for a, dim in zip(arrays, dims)]
    both = jnp.concatenate([t.reshape(len(t), -1) for t in turned], axis=1)
    out, at, outs = (lax.all_gather(both, axis, axis=0, tiled=True), 0, [])
    for t, dim in zip(turned, dims):
        share = out[:, at : at + t[0].size].reshape(-1, *t.shape[1:])
        outs.append(jnp.moveaxis(share, 0, dim))
        at += t[0].size
    return tuple(outs)


def in_blocks(array, dim, devices):
    lengths = array.shape
    blocks = array.reshape(*lengths[:dim], devices, lengths[dim] // devices, *lengths[dim + 1 :])
    return jnp.moveaxis(blocks, dim, 0)


def sent_and_summed(array, axis, dim):
    blocks = in_blocks(array, dim, lax.axis_size(axis))
    arrived = lax.all_to_all(blocks, axis, split_axis=0, concat_axis=0, tiled=True)
    return arrived.astype(jnp.float32).sum(axis=0)


def rms_rows(rows, gain):
    values = rows.astype(jnp.float32)
    scaled = values * lax.rsqrt(jnp.mean(values * values, axis=-1, keepdims=True) + eps)
    return (scaled * gain).astype(jnp.bfloat16)


def body(
    sequence,
    mix_gain,
    ffn_gain,
    proj_outer,
    proj_inner,
    proj_value,
    proj_scales,
    taps,
    mix_out,
    mix_out_scale,
    ffn_gate,
    ffn_up,
    ffn_scales,
    ffn_down,
    down_scale,
):
    local = sequence[0]
    full_rows = lax.all_gather(local, "tp", axis=1, tiled=True)
    normed = rms_rows(full_rows, mix_gain)
    out_scales = gather_turned((mix_out_scale, down_scale), "fs", (0, 0))
    w_outer = proj_outer.astype(jnp.bfloat16)
    w_inner = proj_inner.astype(jnp.bfloat16)
    w_value = proj_value.astype(jnp.bfloat16)
    whole_outer, whole_inner, whole_value = gather_turned(
        (w_outer, w_inner, w_value), "fs", (1, 1, 1)
    )
    outer = jnp.dot(normed, whole_outer, preferred_element_type=jnp.float32)
    inner = jnp.dot(normed, whole_inner, preferred_element_type=jnp.float32)
    value = jnp.dot(normed, whole_value, preferred_element_type=jnp.float32)
    carried = inner * proj_scales[1] * (value * proj_scales[2])
    length = carried.shape[0]
    back_one = jnp.pad(carried, ((1, 0), (0, 0)))[:length]
    back_two = jnp.pad(carried, ((2, 0), (0, 0)))[:length]
    conv = taps[0] * back_two + taps[1] * back_one + taps[2] * carried
    gated = (outer * proj_scales[0] * conv).astype(jnp.bfloat16)
    scale = out_scales[0]
    mixer_terms = (
        jnp.dot(
            gated,
            lax.all_gather(mix_out.astype(jnp.bfloat16), "fs", axis=1, tiled=True),
            preferred_element_type=jnp.float32,
        )
        * scale
    )
    mix = sent_and_summed(mixer_terms.astype(jnp.bfloat16), "tp", 1)
    after = (local.astype(jnp.float32) + mix).astype(jnp.bfloat16)
    after_rows = lax.all_gather(after, "tp", axis=1, tiled=True)
    normed2 = rms_rows(after_rows, ffn_gain)
    w_gate = ffn_gate.astype(jnp.bfloat16)
    w_up = ffn_up.astype(jnp.bfloat16)
    whole_gate, whole_up = gather_turned((w_gate, w_up), "fs", (1, 1))
    gate = jnp.dot(normed2, whole_gate, preferred_element_type=jnp.float32)
    up = jnp.dot(normed2, whole_up, preferred_element_type=jnp.float32)
    hidden = (jax.nn.silu(gate * ffn_scales[0]) * (up * ffn_scales[1])).astype(jnp.bfloat16)
    scale = out_scales[1]
    ffn_terms = (
        jnp.dot(
            hidden,
            lax.all_gather(ffn_down.astype(jnp.bfloat16), "fs", axis=1, tiled=True),
            preferred_element_type=jnp.float32,
        )
        * scale
    )
    ffn = sent_and_summed(ffn_terms.astype(jnp.bfloat16), "tp", 1)
    result = (after.astype(jnp.float32) + ffn).astype(jnp.bfloat16)
    return result[None]


def solution(mesh):
    in_specs = (
        P(("rep", "fs"), None, "tp"),
        P(),
        P(),
        P(None, ("tp", "fs")),
        P(None, ("tp", "fs")),
        P(None, ("tp", "fs")),
        P(None, "tp"),
        P(None, "tp"),
        P("tp", "fs"),
        P("fs"),
        P(None, ("tp", "fs")),
        P(None, ("tp", "fs")),
        P(None, "tp"),
        P("tp", "fs"),
        P("fs"),
    )
    out_specs = P(("rep", "fs"), None, "tp")
    return jax.shard_map(body, mesh=mesh, in_specs=in_specs, out_specs=out_specs, check_vma=False)
```

profile of v0, /device:TPU:1, one launch (start us, length us, event | category | flops | bytes accessed | tf_op | source)
XLA Modules:
  0.0 752.1 jit_solution(7647889185761469245)
XLA Ops:
  6.6 0.0 all-gather.18.cloned.1.call-start
  6.6 0.7 all-gather.18.cloned.1.call-update
  7.3 0.0 all-gather.10.cloned.1.call-start
  7.3 1.0 convert_bitcast_fusion.5
  8.3 1.1 convert_bitcast_fusion.3
  9.4 0.8 pad_maximum_fusion
  10.2 0.0 all-gather.10.cloned.1.call-update
  10.2 0.0 copy-start.12
  10.2 0.0 all-gather.12.cloned.1.call-start
  10.3 0.7 convert_element_type.82
  10.9 0.0 all-gather.12.cloned.1.call-update
  10.9 0.0 all-gather.20.cloned.1.call-start
  11.1 0.8 maximum_bitcast_fusion
  11.9 0.0 all-gather.20.cloned.1.call-update
  11.9 0.0 all-gather.14.cloned.1.call-start
  11.9 0.0 copy-done.11
  12.0 0.0 copy-done.10
  12.0 72.3 %all-gather.1 = f32[32,64,2]{1,2,0:T(2,128)S(1)} all-gather(f32[1,64,2]{1,2,0:T(2,128)S(1)} %maximum_bitcast_fusion.1), channel_id=1, replica_groups=mesh['rep'=2,'fs'=32,'tp'=2] {'fs'}, dimensions={0}, use_global_device_ids=true | all-gather | bytes 16896 | tf_op jit(solution)/shard_map/all_gather | solution.py:12
  84.3 0.1 reshape.42
  84.5 0.0 all-gather.18.cloned.1.call-done
  84.5 2.6 fusion.3
  87.1 100.5 %all-gather.10.cloned.1.call-done = bf16[1024,6144]{1,0:T(8,128)(2,1)} async-done(((bf16[32,6144]{1,0:T(8,128)(2,1)}), bf16[1024,6144]{1,0:T(8,128)(2,1)}) %all-gather.10.cloned.1.call-update) | async-done | bytes 12582928 | tf_op jit(solution)/shard_map/all_gather | solution.py:12
  187.7 6.2 fusion.10
  193.9 7.3 multiply_multiply_fusion
  201.2 140.5 %all-gather.12.cloned.1.call-done = bf16[1024,2048]{0,1:T(8,128)(2,1)} async-done(((bf16[1024,64]{0,1:T(8,128)(2,1)}), bf16[1024,2048]{0,1:T(8,128)(2,1)}) %all-gather.12.cloned.1.call-update) | async-done | bytes 4194320 | tf_op jit(solution)/shard_map/all_gather | solution.py:78
  341.7 15.4 %multiply_convert_fusion.1 = bf16[768,2048]{1,0:T(8,128)(2,1)} fusion(bf16[1024,2048]{0,1:T(8,128)(2,1)} %all-gather.12.cloned.1.call-done, f32[2048]{0:T(1024)S(1)} %bitcast.70, f32[768,1024]{1,0:T(8,128)} %multiply_multiply_fusion, bf16[1024,6144]{1,0:T(8,128)(2,1)} %all-gather.10.cloned.1.call-done, f32[1024]{0:T(1024)S(1)} %bitcast.73, ...), kind=kOutput, calls=%fused_computation.13 | convolution fusion | flops 6458179584 | bytes 17861632 | tf_op jit(solution)/shard_map/dot_general | solution.py:76
  357.1 2.3 copy.25
  359.3 26.6 %all_to_all.10 = bf16[2,768,1024]{2,1,0:T(8,128)(2,1)S(1)} all-to-all(bf16[2,768,1024]{2,1,0:T(8,128)(2,1)S(1)} %bitcast.65), channel_id=1, replica_groups=mesh['rep'=2,'fs'=32,'tp'=2] {'tp'}, dimensions={0} | all-to-all | bytes 6291456 | tf_op jit(solution)/shard_map/all_to_all | solution.py:28
  385.9 0.7 convert_reduce_fusion.1
  386.6 0.7 copy-done
  387.3 1.7 fusion.26
  389.0 0.0 all-gather.14.cloned.1.call-update
  389.1 0.0 all-gather.16.cloned.1.call-start
  389.1 0.7 convert_element_type.94
  389.8 0.0 all-gather.16.cloned.1.call-update
  389.9 0.0 copy-start.13
  389.9 130.2 %all-gather.20.cloned.1.call-done = bf16[32,44,4096]{2,1,0:T(8,128)(2,1)} async-done(((bf16[1,44,4096]{2,1,0:T(8,128)(2,1)}), bf16[32,44,4096]{2,1,0:T(8,128)(2,1)}) %all-gather.20.cloned.1.call-update) | async-done | bytes 11534352 | tf_op jit(solution)/shard_map/all_gather | solution.py:12
  520.1 14.3 %reshape.44 = bf16[1408,4096]{1,0:T(8,128)(2,1)} reshape(bf16[32,44,4096]{2,1,0:T(8,128)(2,1)} %all-gather.20.cloned.1.call-done) | data formatting | bytes 23068672
  534.4 18.9 %all-gather.14.cloned.1.call-done = bf16[768,2048]{1,0:T(8,128)(2,1)} async-done(((bf16[768,1024]{1,0:T(8,128)(2,1)}), bf16[768,2048]{1,0:T(8,128)(2,1)}) %all-gather.14.cloned.1.call-update) | async-done | bytes 3145744 | tf_op jit(solution)/shard_map/all_gather | solution.py:85
  553.3 2.6 fusion
  555.9 9.9 %fusion.6 = f32[768,1408]{1,0:T(8,128)} fusion(bf16[1408,4096]{1,0:T(8,128)(2,1)} %reshape.44, bf16[768,2048]{1,0:T(8,128)(2,1)} %all-gather.14.cloned.1.call-done, f32[2048]{0:T(1024)S(1)} %copy-done.13, f32[768]{0:T(1024)S(1)} %add_rsqrt_fusion), kind=kOutput, calls=%fused_computation.14 | convolution fusion | flops 4435476480 | bytes 13249536 | tf_op jit(solution)/shard_map/dot_general | solution.py:91
  565.8 130.3 %all-gather.16.cloned.1.call-done = bf16[1408,2048]{0,1:T(8,128)(2,1)} async-done(((bf16[1408,64]{0,1:T(8,128)(2,1)}), bf16[1408,2048]{0,1:T(8,128)(2,1)}) %all-gather.16.cloned.1.call-update) | async-done | bytes 5767184 | tf_op jit(solution)/shard_map/all_gather | solution.py:97
  696.1 17.4 %multiply_convert_fusion = bf16[768,2048]{1,0:T(8,128)(2,1)} fusion(bf16[1408,2048]{0,1:T(8,128)(2,1)} %all-gather.16.cloned.1.call-done, f32[2048]{0:T(1024)S(1)} %bitcast.69, f32[768,1408]{1,0:T(8,128)} %fusion.6, bf16[1408,4096]{1,0:T(8,128)(2,1)} %reshape.44, f32[1408]{0:T(1024)S(1)} %get-tuple-element.6, f32[1408]{0:T(1024)S(1)} %get-tuple-element.5, ...), kind=kOutput, calls=%fused_computation.11 | convolution fusion | flops 8876457984 | bytes 22181888 | tf_op jit(solution)/shard_map/dot_general | solution.py:95
  713.5 2.3 copy.24
  715.8 26.0 %all_to_all.11 = bf16[2,768,1024]{2,1,0:T(8,128)(2,1)S(1)} all-to-all(bf16[2,768,1024]{2,1,0:T(8,128)(2,1)S(1)} %bitcast.66), channel_id=1, replica_groups=mesh['rep'=2,'fs'=32,'tp'=2] {'tp'}, dimensions={0} | all-to-all | bytes 6291456 | tf_op jit(solution)/shard_map/all_to_all | solution.py:28
  741.8 0.7 convert_reduce_fusion
  742.5 0.7 copy-done.1
  743.2 2.1 fusion.27
  (31 shorter events, 0.2 us)
Async XLA Ops:
  6.5 3.7 copy-start.6
  6.5 4.4 copy-start.4
  6.5 4.5 copy-start.3
  6.5 5.4 copy-start.11
  6.5 5.4 copy-start.10
  6.5 77.8 %copy-start.8 = (f32[3,1024]{1,0:T(4,128)S(1)}, f32[3,1024]{1,0:T(4,128)}, u32[]{:S(2)}) copy-start(f32[3,1024]{1,0:T(4,128)} %param.21) | copy-start | bytes 36868
  6.6 77.9 %copy-start.9 = (f32[3,1024]{1,0:T(4,128)S(1)}, f32[3,1024]{1,0:T(4,128)}, u32[]{:S(2)}) copy-start(f32[3,1024]{1,0:T(4,128)} %param.22) | copy-start | bytes 36868
  6.6 77.9 %all-gather.18.cloned.1.call-start = ((), (), s32[]{:S(2)}) async-start(), calls=%async_computation.6 | async-start | bytes 4718592 | tf_op jit(solution)/shard_map/all_gather | solution.py:56
  7.3 180.4 %all-gather.10.cloned.1.call-start = ((), (), s32[]{:S(2)}) async-start(), calls=%async_computation.2 | async-start | bytes 12976128 | tf_op jit(solution)/shard_map/all_gather | solution.py:12
  10.2 177.5 %copy-start.12 = (f32[2048]{0:T(1024)S(1)}, f32[2048]{0:T(1024)}, u32[]{:S(2)}) copy-start(f32[2048]{0:T(1024)} %param.16) | copy-start | bytes 24580
  10.2 331.5 %all-gather.12.cloned.1.call-start = ((), (), s32[]{:S(2)}) async-start(), calls=%async_computation.3 | async-start | bytes 4325376 | tf_op jit(solution)/shard_map/all_gather | solution.py:78
  10.9 509.2 %all-gather.20.cloned.1.call-start = ((), (), s32[]{:S(2)}) async-start(), calls=%async_computation.7 | async-start | bytes 12976128 | tf_op jit(solution)/shard_map/all_gather | solution.py:12
  11.9 541.5 %all-gather.14.cloned.1.call-start = ((), (), s32[]{:S(2)}) async-start(), calls=%async_computation.4 | async-start | bytes 4718592 | tf_op jit(solution)/shard_map/all_gather | solution.py:85
  87.1 106.8 %copy-start.2 = (bf16[1,768,2048]{2,1,0:T(8,128)(2,1)S(1)}, bf16[1,768,2048]{2,1,0:T(8,128)(2,1)}, u32[]{:S(2)}) copy-start(bf16[1,768,2048]{2,1,0:T(8,128)(2,1)} %all-gather.18.cloned.1.call-done) | copy-start | bytes 9437188
  385.9 1.4 copy-start
  387.3 1.8 copy-start.5
  387.3 2.5 copy-start.7
  389.1 307.1 %all-gather.16.cloned.1.call-start = ((), (), s32[]{:S(2)}) async-start(), calls=%async_computation.5 | async-start | bytes 5947392 | tf_op jit(solution)/shard_map/all_gather | solution.py:97
  389.9 166.0 %copy-start.13 = (f32[2048]{0:T(1024)S(1)}, f32[2048]{0:T(1024)}, u32[]{:S(2)}) copy-start(f32[2048]{0:T(1024)} %param.17) | copy-start | bytes 24580
  741.8 1.4 copy-start.1
Sparse Core Ops, SparseCore 0:
  9.0 18.4 all-gather.17
  29.2 158.4 all-gather.9
  189.3 152.3 all-gather.11
  343.2 176.8 all-gather.19
  521.6 31.6 all-gather.13
  554.8 141.2 all-gather.15
where the time goes:
time: 753 us; the launch traced here: 752 us
  waiting for transfers between devices  521 us (69%)
  blocking collectives  125 us (17%)
  matrix products  56.2 us (7%)
  local copies, waits for them, and re-layouts  20.5 us (3%)
  other arithmetic  15.4 us (2%)
  between operations  13.7 us (2%)
    all_gather x2, waiting for transfers between devices, gather_turned(): out, at, outs = (lax.all_gather(both, axis, axis=0, tiled=True), 0, [])  231 us
    all_gather x1, waiting for transfers between devices, body(): lax.all_gather(mix_out.astype(jnp.bfloat16), 'fs', axis=1, tiled=True)  140 us
    all_gather x1, waiting for transfers between devices, body(): lax.all_gather(ffn_down.astype(jnp.bfloat16), 'fs', axis=1, tiled=True)  130 us
    all_gather x1, blocking collectives, gather_turned(): out, at, outs = (lax.all_gather(both, axis, axis=0, tiled=True), 0, [])  72.3 us
    all_to_all x2, blocking collectives, sent_and_summed(): lax.all_to_all(blocks, axis, split_axis=0, concat_axis=0, tiled=True)  52.5 us
    all_gather x1, waiting for transfers between devices, body(): after_rows = lax.all_gather(after, 'tp', axis=1, tiled=True)  18.9 us
    dot_general x1, matrix products, body(): jnp.dot(hidden, lax.all_gather(ffn_down.astype(jnp.bfloat16), 'fs', axis=...  17.4 us
    unnamed x30, local copies, waits for them, and re-layouts  15.9 us
  transfers between devices with their start and end apart: 6, of which 5 were waited for; matrix products, arithmetic and copies ran while one was open for 9% of the time, Pallas kernels for 0%

commit v1 on v0

v1 whole, which is shorter than its diff:
```python
import functools

import jax
import jax.numpy as jnp
from jax import lax
from jax.experimental import pallas as pl
from jax.experimental.pallas import tpu as pltpu
from jax.sharding import PartitionSpec as P

F32, BF16 = jnp.float32, jnp.bfloat16
MESH = pl.DeviceIdType.MESH
EPS = 1e-06
D, L, HALF, FFB = 2048, 768, 1024, 48
HALO = 16
UP = L // 2 + HALO
LOW = L // 2
FR = UP + LOW
N_COPIES = 160


def dot_t(a, b):
    return lax.dot_general(a, b, (((1,), (1,)), ((), ())), preferred_element_type=F32)


def kernel(
    seq, wp, wm, wg, wd, taps, out,
    p_all, m_all, g_all, d_all, xo, xf, go, gf, c_s, rs_o, rs_f,
    snd_o, snd_f, rcv_o, rcv_f, keep, fsum, rcv_z, af, hid, fsnd, frcv, res,
    send_sem, recv_sem, loc_sem,
):
    rep, fs, tp = lax.axis_index("rep"), lax.axis_index("fs"), lax.axis_index("tp")
    zl, y, x = fs // 16, (fs // 4) % 4, fs % 4
    z = rep * 2 + zl
    xl, xr, yl, yr = (x + 3) % 4, (x + 1) % 4, (y + 3) % 4, (y + 1) % 4
    xa, ya = (x + 2) % 4, (y + 2) % 4
    zo = 1 - zl

    def plane(yy, xx):
        return {"fs": zl * 16 + yy * 4 + xx}

    def vert(zz):
        return {"rep": zz // 2, "fs": (zz % 2) * 16 + y * 4 + x}

    to_xl, to_xr, to_yl, to_yr = plane(y, xl), plane(y, xr), plane(yl, x), plane(yr, x)
    to_zl, to_zr = vert((z + 3) % 4), vert((z + 1) % 4)
    to_tp = {"tp": 1 - tp}

    count = [0]
    sent = []

    def send(src, dst, dev):
        k = count[0]
        count[0] += 1
        copy = pltpu.make_async_remote_copy(
            src_ref=src, dst_ref=dst, send_sem=send_sem.at[k], recv_sem=recv_sem.at[k],
            device_id=dev, device_id_type=MESH,
        )
        copy.start()
        sent.append(copy)
        return copy

    my_cols = pl.ds(pl.multiple_of(tp * HALF, HALF), HALF)

    local = [
        pltpu.make_async_copy(seq, xo.at[:, my_cols], loc_sem.at[0]),
        pltpu.make_async_copy(wg.at[0], g_all.at[0, zl, y, x], loc_sem.at[1]),
        pltpu.make_async_copy(wp, p_all.at[:, y, x], loc_sem.at[2]),
        pltpu.make_async_copy(wm.at[zl], m_all.at[zl, y, x], loc_sem.at[3]),
        pltpu.make_async_copy(wg.at[1], g_all.at[1, zl, y, x], loc_sem.at[4]),
        pltpu.make_async_copy(wd, d_all.at[zl, y, x], loc_sem.at[5]),
    ]
    for copy in local:
        copy.start()

    barrier = pltpu.get_barrier_semaphore()
    for dev in (to_xl, to_xr, to_yl, to_yr, to_zl, to_zr, to_tp):
        pl.semaphore_signal(barrier, inc=1, device_id=dev, device_id_type=MESH)
    pl.semaphore_wait(barrier, 7)

    class Gather:
        def __init__(self, block, depth):
            self.block, self.q = block, depth // 4
            self.c = {}

        def cols(self, stream, quarter=None):
            start = stream * 2 * self.q
            if quarter is None:
                return pl.ds(start, 2 * self.q)
            return pl.ds(start + quarter * self.q, self.q)

        def pair(self, name, u0, dev0, u1, dev1):
            self.c[name] = (send(u0, u0, dev0), send(u1, u1, dev1))

        def a1(self):
            b = self.block
            u = b(y, x, self.cols(0))
            self.pair("x1", u, to_xr, u, to_xl)
            u = b(y, x, self.cols(1))
            self.pair("y1", u, to_yr, u, to_yl)

        def got(self, name):
            for copy in self.c[name]:
                copy.wait_recv()

        def a2(self):
            b = self.block
            self.got("x1")
            self.pair("x2", b(y, xl, self.cols(0, 0)), to_xr, b(y, xr, self.cols(0, 1)), to_xl)
            self.got("y1")
            self.pair("y2", b(yl, x, self.cols(1, 0)), to_yr, b(yr, x, self.cols(1, 1)), to_yl)

        def a3(self):
            b, every = self.block, slice(None)
            self.got("x2")
            u = b(y, every, self.cols(0))
            self.pair("x3", u, to_yr, u, to_yl)
            self.got("y2")
            u = b(every, x, self.cols(1))
            self.pair("y3", u, to_xr, u, to_xl)

        def a4(self):
            b, every = self.block, slice(None)
            self.got("x3")
            self.pair("x4", b(yl, every, self.cols(0, 0)), to_yr, b(yr, every, self.cols(0, 1)), to_yl)
            self.got("y3")
            self.pair("y4", b(every, xl, self.cols(1, 0)), to_xr, b(every, xr, self.cols(1, 1)), to_xl)

        def a5(self):
            self.got("x4")
            self.got("y4")

        def z_units(self, names):
            b, every = self.block, slice(None)
            for yy, xx in names:
                u = b(yy, every, self.cols(0))
                w = b(every, xx, self.cols(1))
                self.pair(("z", len(self.c)), u, to_zr, w, to_zl)

        def z_own(self):
            self.z_units([(y, x)])

        def z_sides(self):
            self.z_units([(yl, xl), (yr, xr)])

        def z_far(self):
            self.z_units([(ya, xa)])

        def z_got(self):
            for name in list(self.c):
                if name[0] == "z":
                    self.got(name)

    gate = Gather(lambda yy, xx, k: g_all.at[0, zl, yy, xx, :, k], D)
    up = Gather(lambda yy, xx, k: g_all.at[1, zl, yy, xx, :, k], D)
    proj = Gather(lambda yy, xx, k: p_all.at[:, yy, xx, :, k], D)
    mixw = Gather(lambda yy, xx, k: m_all.at[:, yy, xx, :, k], 512)
    down = Gather(lambda yy, xx, k: d_all.at[:, yy, xx, :, k], 32 * FFB)

    local[1].wait()
    gate.a1()
    local[0].wait()
    own = xo.at[:, my_cols]
    row_tp = send(own, own, to_tp)
    row_up = send(xo.at[pl.ds(L - UP, UP), my_cols], xf.at[pl.ds(0, UP), my_cols], to_zr)
    row_low = send(xo.at[pl.ds(0, LOW), my_cols], xf.at[pl.ds(UP, LOW), my_cols], to_zl)
    local[2].wait()
    proj.a1()
    local[3].wait()
    mix_z = (
        send(wm.at[zo, :, pl.ds(0, 256)], m_all.at[zl, y, x, :, pl.ds(0, 256)], to_zr),
        send(wm.at[zo, :, pl.ds(256, 256)], m_all.at[zl, y, x, :, pl.ds(256, 256)], to_zl),
    )
    local[5].wait()
    kd = 16 * FFB
    u0, u1 = d_all.at[zl, y, x, :, pl.ds(0, kd)], d_all.at[zl, y, x, :, pl.ds(kd, kd)]
    down_z = (send(u0, u0, to_zr), send(u1, u1, to_zl))
    local[4].wait()

    def inverse_rms(src, dst, rows, step):
        def one(i, carry):
            at = pl.ds(pl.multiple_of(i * step, step), step)
            v = src[at, :].astype(F32)
            mean = jnp.sum(v * v, axis=-1, keepdims=True) * (1.0 / D)
            dst[at, :] = jnp.broadcast_to(lax.rsqrt(mean + EPS), (step, 128))
            return carry

        lax.fori_loop(0, rows // step, one, 0)

    row_tp.wait_recv()
    inverse_rms(xo, rs_o, L, 16)

    gate.a2()
    proj.a2()
    gate.a3()
    gate.z_own()
    for copy in mix_z:
        copy.wait_recv()
    mixw.a1()
    proj.a3()
    mixw.a2()
    row_up.wait_recv()
    u = xf.at[pl.ds(0, UP), my_cols]
    fwd_up = send(u, u, to_tp)
    row_low.wait_recv()
    u = xf.at[pl.ds(UP, LOW), my_cols]
    fwd_low = send(u, u, to_tp)
    gate.a4()
    gate.z_sides()
    mixw.a3()
    fwd_up.wait_recv()
    fwd_low.wait_recv()
    inverse_rms(xf, rs_f, FR, 16)
    up.a1()
    proj.a4()
    mixw.a4()
    gate.a5()
    gate.z_far()
    up.a2()
    for copy in down_z:
        copy.wait_recv()
    down.a1()
    up.a3()
    up.z_own()
    proj.a5()

    def mixer(rows_ref, rs, dst, groups):
        total = sum(groups)

        def tile(j, carry):
            def part(m):
                w = p_all[m, pl.ds(2 * j, 2)].reshape(256, D)
                return dot_t(rows_ref[...], w)

            r = rs[...]
            r = jnp.concatenate([r, r], axis=1)
            carried = (part(1) * r) * (part(2) * r)
            at = 0
            for g, n in enumerate(groups):
                c_s[pl.ds(at + 8 * g, 8), :] = jnp.zeros((8, 256), F32)
                c_s[pl.ds(at + 8 * g + 8, n), :] = carried[at:at + n]
                at += n
            outer = part(0) * r
            t_cols = pl.ds(pl.multiple_of(zl * 512 + j * 256, 256), 256)
            t0, t1, t2 = taps[0:1, t_cols], taps[1:2, t_cols], taps[2:3, t_cols]
            at = 0
            d_cols = pl.ds(pl.multiple_of(j * 256, 256), 256)
            for g, n in enumerate(groups):
                first = at + 8 * g + 8
                conv = (
                    t0 * c_s[pl.ds(first - 2, n), :]
                    + t1 * c_s[pl.ds(first - 1, n), :]
                    + t2 * c_s[pl.ds(first, n), :]
                )
                dst[pl.ds(at, n), d_cols] = (outer[at:at + n] * conv).astype(BF16)
                at += n
            return carry

        lax.fori_loop(0, 2, tile, 0)

    mixer(xf, rs_f, gf, (UP, LOW))
    up.a4()
    up.z_sides()
    down.a2()
    mixer(xo, rs_o, go, (L,))
    mixw.a5()
    down.a3()

    f_rows = pl.ds(HALO, L)
    cols = [pl.ds(j * 256, 256) for j in range(4)]

    def mtile(zz, j):
        return m_all[zz, j].reshape(256, 512)

    ex_f, ex_o = [], []
    for j in range(4):
        snd_f[:, cols[j]] = dot_t(gf[f_rows, :], mtile(1 - tp, j)).astype(BF16)
        ex_f.append(send(snd_f.at[:, cols[j]], rcv_f.at[:, cols[j]], to_tp))
    home = []
    for j in range(4):
        v = dot_t(gf[f_rows, :], mtile(tp, j))
        ex_f[j].wait_recv()
        fsum[:, cols[j]] = (v + rcv_f[:, cols[j]].astype(F32)).astype(BF16)
        a, b = pl.ds(0, LOW), pl.ds(LOW, LOW)
        home.append(send(fsum.at[a, cols[j]], rcv_z.at[b, cols[j]], to_zl))
        home.append(send(fsum.at[b, cols[j]], rcv_z.at[a, cols[j]], to_zr))
    up.a5()
    up.z_far()
    for j in range(4):
        snd_o[:, cols[j]] = dot_t(go[...], mtile(1 - tp, j)).astype(BF16)
        ex_o.append(send(snd_o.at[:, cols[j]], rcv_o.at[:, cols[j]], to_tp))
    for j in range(4):
        keep[:, cols[j]] = dot_t(go[...], mtile(tp, j))
    down.a4()
    ex_a = []
    for j in range(4):
        ex_o[j].wait_recv()
        home[2 * j].wait_recv()
        home[2 * j + 1].wait_recv()
        a_cols = pl.ds(pl.multiple_of(tp * HALF + j * 256, 256), 256)
        after = (
            xo[:, a_cols].astype(F32)
            + (keep[:, cols[j]] + rcv_o[:, cols[j]].astype(F32))
            + rcv_z[:, cols[j]].astype(F32)
        )
        af[:, a_cols] = after.astype(BF16)
        ex_a.append(send(af.at[:, a_cols], af.at[:, a_cols], to_tp))
    for copy in ex_a:
        copy.wait_recv()
    inverse_rms(af, rs_o, L, 16)

    gate.z_got()
    up.z_got()
    g_flat = g_all.reshape(2, 32 * FFB, D)

    def ffn_tile(t, carry):
        at = pl.ds(pl.multiple_of(t * 256, 256), 256)
        r = rs_o[...]
        r = jnp.concatenate([r, r], axis=1)
        g = dot_t(af[...], g_flat[0, at, :]) * r
        u = dot_t(af[...], g_flat[1, at, :]) * r
        hid[:, at] = (g / (1.0 + jnp.exp(-g)) * u).astype(BF16)
        return carry

    lax.fori_loop(0, 6, ffn_tile, 0)

    down.a5()

    def dtile(zz, j):
        return d_all[zz, j].reshape(256, 32 * FFB)

    ex_h = []
    for j in range(4):
        fsnd[:, cols[j]] = dot_t(hid[...], dtile(1 - tp, j)).astype(BF16)
        ex_h.append(send(fsnd.at[:, cols[j]], frcv.at[:, cols[j]], to_tp))
    back = []
    for j in range(4):
        v = dot_t(hid[...], dtile(tp, j))
        ex_h[j].wait_recv()
        a_cols = pl.ds(pl.multiple_of(tp * HALF + j * 256, 256), 256)
        total = af[:, a_cols].astype(F32) + (v + frcv[:, cols[j]].astype(F32))
        res[:, cols[j]] = total.astype(BF16)
        back.append(pltpu.make_async_copy(res.at[:, cols[j]], out.at[:, cols[j]], loc_sem.at[j]))
        back[-1].start()
    for copy in back:
        copy.wait()
    for copy in sent:
        copy.wait_send()


def body(
    sequence, mix_gain, ffn_gain, proj_outer, proj_inner, proj_value, proj_scales, taps,
    mix_out, mix_out_scale, ffn_gate, ffn_up, ffn_scales, ffn_down, down_scale,
):
    fs = lax.axis_index("fs")
    scales = lax.dynamic_slice(proj_scales, (0, fs * 32), (3, 32))
    wp = jnp.stack(
        [
            (w * mix_gain[:, None] * scales[i][None, :]).astype(BF16).T
            for i, w in enumerate((proj_outer, proj_inner, proj_value))
        ]
    )
    wm = (mix_out * mix_out_scale[None, :]).astype(BF16).T
    wm = jnp.moveaxis(wm.reshape(64, 2, 512), 1, 0)
    f_scales = lax.dynamic_slice(ffn_scales, (0, fs * 44), (2, 44))
    wg = jnp.stack(
        [
            (w * ffn_gain[:, None] * f_scales[i][None, :]).astype(BF16).T
            for i, w in enumerate((ffn_gate, ffn_up))
        ]
    )
    wg = jnp.pad(wg, ((0, 0), (0, FFB - 44), (0, 0)))
    wd = (ffn_down * down_scale[None, :]).astype(BF16).T
    wd = jnp.pad(wd.reshape(64, 32, 44), ((0, 0), (0, 0), (0, FFB - 44))).reshape(64, 32 * FFB)

    vm = pltpu.VMEM
    result = pl.pallas_call(
        kernel,
        out_shape=jax.ShapeDtypeStruct((L, HALF), BF16),
        in_specs=[pl.BlockSpec(memory_space=pl.ANY)] * 5 + [pl.BlockSpec(memory_space=vm)],
        out_specs=pl.BlockSpec(memory_space=pl.ANY),
        scratch_shapes=[
            vm((3, 4, 4, 32, D), BF16),
            vm((2, 4, 4, 64, 512), BF16),
            vm((2, 2, 4, 4, FFB, D), BF16),
            vm((2, 4, 4, 64, 32 * FFB), BF16),
            vm((L, D), BF16),
            vm((FR, D), BF16),
            vm((L, 512), BF16),
            vm((FR, 512), BF16),
            vm((FR + 16, 256), F32),
            vm((L, 128), F32),
            vm((FR, 128), F32),
            vm((L, HALF), BF16),
            vm((L, HALF), BF16),
            vm((L, HALF), BF16),
            vm((L, HALF), BF16),
            vm((L, HALF), F32),
            vm((L, HALF), BF16),
            vm((L, HALF), BF16),
            vm((L, D), BF16),
            vm((L, 32 * FFB), BF16),
            vm((L, HALF), BF16),
            vm((L, HALF), BF16),
            vm((L, HALF), BF16),
            pltpu.SemaphoreType.DMA((N_COPIES,)),
            pltpu.SemaphoreType.DMA((N_COPIES,)),
            pltpu.SemaphoreType.DMA((6,)),
        ],
        compiler_params=pltpu.CompilerParams(
            collective_id=0, has_side_effects=True, vmem_limit_bytes=67_000_000
        ),
        name="layer",
    )(sequence[0], wp, wm, wg, wd, taps)
    return result[None]


def solution(mesh):
    in_specs = (
        P(("rep", "fs"), None, "tp"),
        P(),
        P(),
        P(None, ("tp", "fs")),
        P(None, ("tp", "fs")),
        P(None, ("tp", "fs")),
        P(None, "tp"),
        P(None, "tp"),
        P("tp", "fs"),
        P("fs"),
        P(None, ("tp", "fs")),
        P(None, ("tp", "fs")),
        P(None, "tp"),
        P("tp", "fs"),
        P("fs"),
    )
    out_specs = P(("rep", "fs"), None, "tp")
    return jax.shard_map(body, mesh=mesh, in_specs=in_specs, out_specs=out_specs, check_vma=False)
```

time: 753 us -> 169 us (0.22)
  waiting for transfers between devices: 521 us -> 0 us
  Pallas kernels: 0 us -> 158 us
  blocking collectives: 125 us -> 0 us
  matrix products: 56.2 us -> 0 us
  between operations: 13.7 us -> 0.09 us
  local copies, waits for them, and re-layouts: 20.5 us -> 7.26 us
  other arithmetic: 15.4 us -> 4.01 us
    all_gather x6 -> x0, waiting for transfers between devices: 520 us -> none  [the longest x2 231 us: gather_turned(): out, at, outs = (lax.all_gather(both, axis, axis=0, tiled=True), 0, [])]
    pallas_call x0 -> x1, Pallas kernels: none -> 158 us  [body(): pl.pallas_call(kernel, out_shape=jax.ShapeDtypeStruct((L, HALF), BF16), i...]
    all_gather x1 -> x0, blocking collectives: 72.3 us -> none  [gather_turned(): out, at, outs = (lax.all_gather(both, axis, axis=0, tiled=True), 0, [])]
    dot_general x5 -> x0, matrix products: 56.2 us -> none  [the longest x1 17.4 us: body(): jnp.dot(hidden, lax.all_gather(ffn_down.astype(jnp.bfloat16), 'fs', axis=...]
    all_to_all x2 -> x0, blocking collectives: 52.5 us -> none  [sent_and_summed(): lax.all_to_all(blocks, axis, split_axis=0, concat_axis=0, tiled=True)]
    unnamed x30 -> x17, local copies, waits for them, and re-layouts: 15.9 us -> 2.71 us
  transfers between devices with their start and end apart: 6 -> 0, of which waited for: 5 -> 0; matrix products, arithmetic and copies ran while one was open for 9% -> 0% of each run, Pallas kernels for 0% -> 0%
where the time goes in v1:
time: 169 us
  Pallas kernels  158 us (93%)
  local copies, waits for them, and re-layouts  7.26 us (4%)
  other arithmetic  4.01 us (2%)
    pallas_call x1, Pallas kernels, body(): pl.pallas_call(kernel, out_shape=jax.ShapeDtypeStruct((L, HALF), BF16), i...  158 us

profile of v1, /device:TPU:1, one launch (start us, length us, event | category | flops | bytes accessed | tf_op | source)
XLA Modules:
  0.0 168.9 jit_solution(2178270477442259961)
XLA Ops:
  0.0 0.0 copy-start
  0.0 0.8 constant_dynamic-slice_fusion
  0.8 0.0 copy-done
  0.8 0.1 constant_dynamic-slice_fusion.1
  0.9 1.0 multiply_convert_fusion.3
  1.9 0.7 copy.19
  2.6 0.0 copy-start.3
  2.6 0.0 copy-start.4
  2.6 0.0 copy-start.5
  2.6 0.0 copy-start.6
  2.6 1.1 fusion.5
  3.7 1.5 reshape.14
  5.2 0.1 pad.9
  5.3 0.0 copy-start.1
  5.3 0.0 copy-start.2
  5.3 0.0 copy-start.7
  5.3 1.5 reshape.15.wd
  6.8 0.0 copy-done.3
  6.8 0.0 copy-done.4
  6.8 0.0 copy-done.5
  6.8 0.0 copy-done.6
  6.8 0.1 fusion.6
  7.0 0.8 pad_maximum_fusion.wp
  7.8 0.0 copy-done.1
  7.8 0.0 copy-done.2
  7.8 0.0 copy-done.7
  7.8 0.1 fusion.3
  7.9 0.8 fusion.2.wg
  8.7 157.6 %layer.1 = bf16[768,1024]{1,0:T(8,128)(2,1)} custom-call(bf16[768,1024]{1,0:T(8,128)(2,1)} %bitcast.43, bf16[3,32,2048]{2,1,0:T(8,128)(2,1)} %pad_maximum_fusion.wp, bf16[2,64,512]{2,1,0:T(8,128)(2,1)} %bitcast.44, bf16[2,48,2048]{2,1,0:T(8,128)(2,1)} %fusion.2.wg, bf16[64,1536]{1,0:T(8,128)(2,1)} %reshape.15.wd, f32[3,1024]{1,0:T(4,128)} %taps.1), custom_call_target="tpu_custom_call" | custom-call | tf_op jit(solution)/shard_map/layer/pallas_call | solution.py:376
  166.3 2.7 %copy.21 = bf16[1,768,1024]{2,1,0:T(8,128)(2,1)} copy(bf16[1,768,1024]{2,1,0:T(8,128)(2,1)} %bitcast.42) | data formatting | bytes 3145728
  (2 shorter events, 0.0 us)
Async XLA Ops:
  0.0 0.8 copy-start
  2.6 4.3 %copy-start.3 = (f32[2048,32]{0,1:T(8,128)S(1)}, f32[2048,32]{0,1:T(8,128)}, u32[]{:S(2)}) copy-start(f32[2048,32]{0,1:T(8,128)} %param.18) | copy-start | bytes 786436
  2.6 4.3 %copy-start.4 = (f32[2048,32]{0,1:T(8,128)S(1)}, f32[2048,32]{0,1:T(8,128)}, u32[]{:S(2)}) copy-start(f32[2048,32]{0,1:T(8,128)} %param.19) | copy-start | bytes 786436
  2.6 4.3 %copy-start.5 = (f32[2048,32]{0,1:T(8,128)S(1)}, f32[2048,32]{0,1:T(8,128)}, u32[]{:S(2)}) copy-start(f32[2048,32]{0,1:T(8,128)} %param.20) | copy-start | bytes 786436
  2.6 4.3 %copy-start.6 = (f32[2048]{0:T(1024)S(1)}, f32[2048]{0:T(1024)}, u32[]{:S(2)}) copy-start(f32[2048]{0:T(1024)} %param.16) | copy-start | bytes 24580
  5.3 2.5 %copy-start.1 = (f32[2048,44]{0,1:T(8,128)S(1)}, f32[2048,44]{0,1:T(8,128)}, u32[]{:S(2)}) copy-start(f32[2048,44]{0,1:T(8,128)} %param.25) | copy-start | bytes 1081348
  5.3 2.4 %copy-start.2 = (f32[2048,44]{0,1:T(8,128)S(1)}, f32[2048,44]{0,1:T(8,128)}, u32[]{:S(2)}) copy-start(f32[2048,44]{0,1:T(8,128)} %param.26) | copy-start | bytes 1081348
  5.3 2.4 %copy-start.7 = (f32[2048]{0:T(1024)S(1)}, f32[2048]{0:T(1024)}, u32[]{:S(2)}) copy-start(f32[2048]{0:T(1024)} %param.17) | copy-start | bytes 24580
